TPU v7x, 32 devices: a whole 2x2x4 slice. The times are simulated.
32 devices in a mesh: ep: 16 (over z, y, x), tp: 2 (over core).
Axes of the slice: x: 2, y: 2, z: 4, core: 2. Of those that a mesh axis runs over, the one named last changes fastest.
Arguments:
- tokens: bfloat16 [384, 2048], P('ep'), may hold values from -6 to 6
- norm_gain: bfloat16 [2048], replicated, may hold values from 0.099609375 to 1.8984375
- query_w: bfloat16 [2048, 1024], P(None, 'tp'), may hold values from -0.125 to 0.125
- key_w: bfloat16 [2048, 128], replicated, may hold values from -0.125 to 0.125
- value_w: bfloat16 [2048, 128], replicated, may hold values from -0.125 to 0.125
- forget_w: bfloat16 [2048, 16], replicated, may hold values from -0.125 to 0.125
- forget_bias: float32 [16], replicated, may hold values from 0 to 4
- query_gain: bfloat16 [64], replicated, may hold values from 0.099609375 to 1.8984375
- key_gain: bfloat16 [64], replicated, may hold values from 0.099609375 to 1.8984375
- cache_key: bfloat16 [384, 2, 64, 1024], P('ep', 'tp'), may hold values from -6 to 6
- cache_value: bfloat16 [384, 2, 64, 1024], P('ep', 'tp'), may hold values from -6 to 6
- cache_gate: float32 [384, 16, 1024], P('ep', 'tp'), may hold values from -105 to 0, as said below
- cache_len: int32 [384], P('ep'), may hold values from 256 to 1024
- out_w: bfloat16 [1024, 2048], P('tp'), may hold values from -0.1875 to 0.1875
- post_gain: bfloat16 [2048], replicated, may hold values from 0.099609375 to 1.8984375
- branch_gate: bfloat16 [2048], replicated, may hold values from -0.125 to 0.125
- dense_gate_w: bfloat16 [2048, 16384], P(None, ('ep', 'tp')), may hold values from -0.125 to 0.125
- dense_up_w: bfloat16 [2048, 16384], P(None, ('ep', 'tp')), may hold values from -1.3258252 to 1.3258252
- dense_down_w: bfloat16 [16384, 2048], P(('ep', 'tp')), may hold values from -0.046875 to 0.046875
- expert_choice: int32 [384, 2], P('ep'), may hold values from 0 to 15, as said below
- route_weight: float32 [384, 2], P('ep'), may hold values from 0.1 to 1
- expert_gate_w: bfloat16 [16, 2048, 1024], P('ep', None, 'tp'), may hold values from -0.125 to 0.125
- expert_up_w: bfloat16 [16, 2048, 1024], P('ep', None, 'tp'), may hold values from -0.125 to 0.125
- expert_down_w: bfloat16 [16, 1024, 2048], P('ep', 'tp'), may hold values from -0.1875 to 0.1875
Outputs:
- mixed_out: bfloat16 [384, 2048], P('ep', 'tp')
- fresh_key: bfloat16 [384, 2, 64], P('ep', 'tp')
- fresh_value: bfloat16 [384, 2, 64], P('ep', 'tp')
- fresh_gate: float32 [384, 16], P('ep', 'tp')
Inputs may be any that keep to these rules, and one draw needn't show every extreme that they name: `cache_gate`: Non-increasing along positions. `expert_choice`: experts 4 * g to 4 * g + 3 form group g. A token names 2 different experts of one group. Among the 24 tokens of one index of ep, those at even offsets all choose one group and the others choose other groups; no expert is named more than 6 times by them, and some expert exactly 6 times.
All inputs are finite; a program needn't handle non-finite values.
Results may differ from a plain program's by a relative error of at most 0.014.
Values may be sent and summed in bfloat16 or wider, within the bound.
A program may use at most 128 MiB of HBM per device.

v0:
```python
import jax
import jax.numpy as jnp
from jax import lax
from jax.sharding import PartitionSpec as P

FF2 = 16384
GROUPS = 4
norm_eps = 1e-06


def rms_scale(values, gain_vec):
    mean_square = jnp.mean(values * values, axis=-1, keepdims=True)
    return values * lax.rsqrt(mean_square + norm_eps) * gain_vec


def rounded(values):
    return lax.optimization_barrier(values.astype(jnp.bfloat16)).astype(jnp.float32)


def swiglu_rows(inputs, gate_weight, up_weight):
    gate_value = jnp.dot(inputs, gate_weight, preferred_element_type=jnp.float32)
    up_value = jnp.dot(inputs, up_weight, preferred_element_type=jnp.float32)
    return jax.nn.silu(gate_value) * up_value


def flat_terms(hidden, down_weight, ep_count, tp_count, seq_count):
    spread_hidden = hidden.astype(jnp.bfloat16).reshape(ep_count, seq_count, -1)
    split_down = down_weight.reshape(down_weight.shape[0], tp_count, -1)
    return jnp.einsum(
        "esh,hcd->ecsd", spread_hidden, split_down, preferred_element_type=jnp.float32
    )


def body(
    tokens,
    norm_gain,
    query_w,
    key_w,
    value_w,
    forget_w,
    forget_bias,
    query_gain,
    key_gain,
    cache_key,
    cache_value,
    cache_gate,
    cache_len,
    out_w,
    post_gain,
    branch_gate,
    dense_gate_w,
    dense_up_w,
    dense_down_w,
    expert_choice,
    route_weight,
    expert_gate_w,
    expert_up_w,
    expert_down_w,
):
    seq_count = tokens.shape[0]
    model_width = tokens.shape[1]
    heads_local = cache_gate.shape[1]
    kv_local = cache_key.shape[1]
    head_size = cache_key.shape[2]
    cache_span = cache_key.shape[3]
    tp_count = lax.axis_size("tp")
    ep_count = lax.axis_size("ep")
    tp_rank = lax.axis_index("tp")
    half_width = model_width // tp_count
    score_scale = head_size ** (-0.5)
    resid_in = tokens.astype(jnp.float32)
    normed = rms_scale(resid_in, norm_gain.astype(jnp.float32)).astype(jnp.bfloat16)
    queries = jnp.dot(normed, query_w, preferred_element_type=jnp.float32).reshape(
        seq_count, heads_local, head_size
    )
    queries = rms_scale(queries, query_gain.astype(jnp.float32)).astype(jnp.bfloat16)
    keys_all = jnp.dot(normed, key_w, preferred_element_type=jnp.float32).reshape(
        seq_count, -1, head_size
    )
    keys_all = rms_scale(keys_all, key_gain.astype(jnp.float32)).astype(jnp.bfloat16)
    values_all = (
        jnp.dot(normed, value_w, preferred_element_type=jnp.float32)
        .astype(jnp.bfloat16)
        .reshape(seq_count, -1, head_size)
    )
    fresh_key = lax.dynamic_slice_in_dim(keys_all, tp_rank * kv_local, kv_local, 1)
    fresh_value = lax.dynamic_slice_in_dim(values_all, tp_rank * kv_local, kv_local, 1)
    forget_all = jax.nn.log_sigmoid(
        jnp.dot(normed, forget_w, preferred_element_type=jnp.float32) + forget_bias
    )
    log_forget = lax.dynamic_slice_in_dim(forget_all, tp_rank * heads_local, heads_local, 1)
    repeat = heads_local // kv_local
    grouped = queries.reshape(seq_count, kv_local, repeat, head_size)
    scores = (
        jnp.einsum("sgrd,sgdl->sgrl", grouped, cache_key, preferred_element_type=jnp.float32)
        * score_scale
    )
    own_score = (
        jnp.einsum("sgrd,sgd->sgr", grouped, fresh_key, preferred_element_type=jnp.float32)
        * score_scale
    )
    current_slot_offset = lax.broadcasted_iota(jnp.int32, (seq_count, cache_span), 1)
    at_last = (current_slot_offset == cache_len[:, None] - 1)[:, None, :]
    previous = jnp.sum(jnp.where(at_last, cache_gate, jnp.zeros_like(cache_gate)), axis=2)
    current = previous + log_forget
    decay_bias = (current[:, :, None] - cache_gate).reshape(seq_count, kv_local, repeat, cache_span)
    is_valid = (current_slot_offset < cache_len[:, None])[:, None, None, :]
    logits = jnp.where(is_valid, scores + decay_bias, -jnp.inf)
    top_logit = jnp.maximum(jnp.max(logits, axis=3), own_score)
    weights = jnp.exp(logits - top_logit[..., None])
    own_weight = jnp.exp(own_score - top_logit)
    total_weight = jnp.sum(weights, axis=3) + own_weight
    cache_probs = (weights / total_weight[..., None]).astype(jnp.bfloat16)
    own_prob = (own_weight / total_weight).astype(jnp.bfloat16)
    mixed_heads = jnp.einsum(
        "sgrl,sgdl->sgrd", cache_probs, cache_value, preferred_element_type=jnp.float32
    )
    mixed_heads = (
        mixed_heads
        + own_prob.astype(jnp.float32)[..., None] * fresh_value.astype(jnp.float32)[:, :, None, :]
    )
    attn_heads = mixed_heads.reshape(seq_count, heads_local * head_size).astype(jnp.bfloat16)
    partial_value = jnp.dot(attn_heads, out_w, preferred_element_type=jnp.float32)
    attn_sum = lax.psum(partial_value.astype(jnp.bfloat16), "tp").astype(jnp.float32)
    resid_out = rounded(resid_in + attn_sum)
    post_norm = rms_scale(resid_out, post_gain.astype(jnp.float32)).astype(jnp.bfloat16)
    branch = jax.nn.sigmoid(jnp.dot(post_norm, branch_gate, preferred_element_type=jnp.float32))
    all_tokens = lax.all_gather(post_norm, "ep", axis=0, tiled=True)
    hidden = swiglu_rows(all_tokens, dense_gate_w, dense_up_w)
    squares = jnp.sum(hidden * hidden, axis=1)
    dense_terms = flat_terms(hidden, dense_down_w, ep_count, tp_count, seq_count)
    spread = jnp.broadcast_to(
        squares.reshape(ep_count, 1, seq_count), (ep_count, tp_count, seq_count)
    ).reshape(-1)
    dense_sum, square_sum = (
        lax.psum_scatter(
            dense_terms.reshape(-1, half_width), ("ep", "tp"), scatter_dimension=0, tiled=True
        ),
        lax.psum_scatter(spread, ("ep", "tp"), scatter_dimension=0, tiled=True),
    )
    dense_out = rounded(dense_sum * lax.rsqrt(square_sum / FF2 + norm_eps)[:, None])
    per_group = ep_count // GROUPS
    capacity = 2 * ((seq_count + 2 * per_group - 1) // (2 * per_group))
    route_count = expert_choice.shape[1]
    route_ids = expert_choice.reshape(-1)
    member = (route_ids[:, None] == jnp.arange(ep_count)[None, :]).astype(jnp.int32)
    slot_index = jnp.sum((jnp.cumsum(member, axis=0) - member) * member, axis=1)
    target = (route_ids * capacity + slot_index).reshape(seq_count, route_count)
    place_map = (target[:, :, None] == jnp.arange(ep_count * capacity)[None, None, :]).astype(
        jnp.bfloat16
    )
    outgoing = jnp.einsum("skc,sd->cd", place_map, post_norm, preferred_element_type=jnp.float32)
    outgoing = outgoing.astype(jnp.bfloat16).reshape(ep_count, capacity, model_width)
    arrived = lax.all_to_all(outgoing, "ep", split_axis=0, concat_axis=0, tiled=True)
    item_count = arrived.shape[1]
    slot_rows = arrived.reshape(-1, model_width)
    activated = swiglu_rows(slot_rows, expert_gate_w[0], expert_up_w[0]).astype(jnp.bfloat16)
    partial_out = jnp.dot(activated, expert_down_w[0], preferred_element_type=jnp.float32)
    partial_out = partial_out.reshape(ep_count, item_count, model_width)
    halves = lax.psum_scatter(
        partial_out.astype(jnp.bfloat16), "tp", scatter_dimension=2, tiled=True
    )
    returned = lax.all_to_all(halves, "ep", split_axis=0, concat_axis=0, tiled=True).reshape(
        ep_count * capacity, half_width
    )
    routed = jnp.einsum("skc,cd->skd", place_map, returned, preferred_element_type=jnp.float32)
    expert_sum = jnp.sum(route_weight[:, :, None] * routed, axis=1)
    resid_columns = lax.dynamic_slice_in_dim(resid_out, tp_rank * half_width, half_width, 1)
    mixed_out = (resid_columns + expert_sum + branch[:, None] * dense_out).astype(jnp.bfloat16)
    return (mixed_out, fresh_key, fresh_value, current)


def solution(mesh):
    placed = (
        P("ep", None),
        P(),
        P(None, "tp"),
        P(),
        P(),
        P(),
        P(),
        P(),
        P(),
        P("ep", "tp", None, None),
        P("ep", "tp", None, None),
        P("ep", "tp", None),
        P("ep"),
        P("tp", None),
        P(),
        P(),
        P(None, ("ep", "tp")),
        P(None, ("ep", "tp")),
        P(("ep", "tp"), None),
        P("ep", None),
        P("ep", None),
        P("ep", None, "tp"),
        P("ep", None, "tp"),
        P("ep", "tp", None),
    )
    return jax.shard_map(
        body,
        mesh=mesh,
        in_specs=placed,
        out_specs=(P("ep", "tp"), P("ep", "tp", None), P("ep", "tp", None), P("ep", "tp")),
        check_vma=False,
    )
```

profile of v0, /device:TPU:0, one launch (start us, length us, event | category | flops | bytes accessed | tf_op | source)
XLA Modules:
  0.0 239.2 jit_solution(11453295453262258375)
XLA Ops:
  8.1 0.9 iota_compare_fusion.1
  9.0 1.3 select_reduce_fusion
  11.1 1.0 fusion.41
  12.2 1.2 fusion.68
  13.4 2.1 fusion.66
  15.8 1.3 fusion.63
  17.7 1.9 fusion.69
  21.8 3.1 %fusion.30 = bf16[24,8,64]{2,1,0:T(8,128)(2,1)S(1)} fusion(bf16[24,1,64,1024]{3,2,1,0:T(8,128)(2,1)} %param.34, f32[24,8,1024]{2,1,0:T(8,128)} %copy-done.1, f32[24,8]{1,0:T(8,128)S(1)} %get-tuple-element.9, f32[24,8]{1,0:T(8,128)S(1)} %multiply_maximum_fusion, f32[24,64]{1,0:T(8,128)S(1)} %get-tuple-element.4, f32[24,8]{1,0:T(8,128)S(1)} %get-tuple-element.8), kind=kOutput, calls=%fused_computation.24 | convolution fusion | flops 25792512 | bytes 3965184 | tf_op jit(solution)/shard_map/sgrl,sgdl->sgrd/dot_general | solution.py:115
  25.0 2.6 %convolution_convert_fusion.2 = bf16[24,2048]{1,0:T(8,128)(2,1)} fusion(bf16[24,512]{1,0:T(8,128)(2,1)S(1)} %convert_element_type.106, bf16[512,2048]{1,0:T(8,128)(2,1)} %param.37), kind=kOutput, calls=%fused_computation.6 | convolution fusion | flops 50380800 | bytes 2220032 | tf_op jit(solution)/shard_map/dot_general | solution.py:123
  27.7 20.6 %all-reduce.3.cloned.1.call-done = bf16[24,2048]{1,0:T(8,128)(2,1)} async-done(((bf16[24,2048]{1,0:T(8,128)(2,1)}), bf16[24,2048]{1,0:T(8,128)(2,1)}) %all-reduce.3.cloned.1.call-update) | async-done | bytes 98320 | tf_op jit(solution)/shard_map/psum | solution.py:124
  48.4 0.9 fusion.44
  51.5 1.2 fusion.71
  52.7 0.9 reshape.193
  53.6 24.4 %all_to_all.10 = bf16[16,6,2048]{2,1,0:T(8,128)(2,1)} all-to-all(bf16[16,6,2048]{2,1,0:T(8,128)(2,1)} %reshape.193), channel_id=1, replica_groups=mesh['ep'=16,'tp'=2] {'ep'}, dimensions={0} | all-to-all | bytes 786432 | tf_op jit(solution)/shard_map/all_to_all | solution.py:154
  78.1 1.2 reshape.194
  79.3 2.2 fusion.9
  81.5 1.1 fusion.24
  82.6 0.9 dot_general.64
  83.5 2.8 %convolution_convert_fusion = bf16[16,6,2048]{2,0,1:T(8,128)(2,1)} fusion(bf16[1,512,2048]{2,1,0:T(8,128)(2,1)} %param.47, bf16[16,6,512]{2,1,0:T(8,128)(2,1)S(1)} %dot_general.64), kind=kOutput, calls=%fused_computation.4 | convolution fusion | flops 201523200 | bytes 2588672 | tf_op jit(solution)/shard_map/dot_general | solution.py:158
  86.4 26.2 %all-gather.2.cloned.1.call-done = bf16[384,2048]{1,0:T(8,128)(2,1)} async-done(((bf16[24,2048]{1,0:T(8,128)(2,1)}), bf16[384,2048]{1,0:T(8,128)(2,1)}) %all-gather.2.cloned.1.call-update) | async-done | bytes 1572880 | tf_op jit(solution)/shard_map/all_gather | solution.py:128
  112.6 3.2 %fusion.70 = f32[384,512]{1,0:T(8,128)S(1)} fusion(bf16[384,2048]{1,0:T(8,128)(2,1)} %all-gather.2.cloned.1.call-done, bf16[2048,512]{1,0:T(8,128)(2,1)} %param.40), kind=kOutput, calls=%fused_computation.98 | convolution fusion | flops 805306368 | bytes 4456448 | tf_op jit(solution)/shard_map/dot_general | solution.py:21
  115.8 1.1 multiply_reduce_fusion
  117.4 2.7 %fusion.4 = f32[16,24,2,1024]{3,1,2,0:T(8,128)} fusion(bf16[16,24,512,1]{2,1,3,0:T(8,128)(2,1)S(1)} %bitcast.85, bf16[64,2,8,1024]{3,2,1,0:T(8,128)(2,1)S(1)} %bitcast.84), kind=kOutput, calls=%fused_computation.8 | convolution fusion | flops 805306368 | bytes 5636096 | tf_op jit(solution)/shard_map/esh,hcd->ecsd/dot_general | solution.py:29
  121.4 1.8 copy.67
  123.1 6.8 %all-to-all-start.1 = ((bf16[16,6,1024]{2,1,0:T(8,128)(2,1)}), bf16[16,6,1024]{2,1,0:T(8,128)(2,1)S(1)}, u32[]{:S(2)}, u32[]{:S(2)}) async-start(bf16[16,6,1024]{2,1,0:T(8,128)(2,1)} %copy.67), calls=%async_computation.2 | async-start | bytes 524288 | tf_op jit(solution)/shard_map/all_to_all | solution.py:163
  131.3 1.0 fusion.37
  132.3 7.9 %all-to-all-done.1 = bf16[16,6,1024]{2,1,0:T(8,128)(2,1)S(1)} async-done(((bf16[16,6,1024]{2,1,0:T(8,128)(2,1)}), bf16[16,6,1024]{2,1,0:T(8,128)(2,1)S(1)}, u32[]{:S(2)}, u32[]{:S(2)}) %all-to-all-start.1) | async-done | bytes 196640 | tf_op jit(solution)/shard_map/all_to_all | solution.py:163
  141.0 1.2 fusion.23
  142.4 38.9 %all-reduce = f32[768]{0:T(1024)S(1)} all-reduce(f32[768]{0:T(1024)S(1)} %reshape.199), channel_id=4, replica_groups=mesh['ep'=16,'tp'=2] {'ep','tp'}, use_global_device_ids=true, to_apply=%region_15.16.clone | all-reduce | flops 768 | bytes 6144
  181.4 48.7 %reduce-scatter.5.cloned.1.call-done = f32[24,1024]{1,0:T(8,128)} async-done(((f32[768,1024]{1,0:T(8,128)}), f32[24,1024]{1,0:T(8,128)}) %reduce-scatter.5.cloned.1.call-update) | async-done | bytes 98320 | tf_op jit(solution)/shard_map/reduce_scatter | solution.py:136
  230.1 1.0 multiply_convert_fusion.1
  231.1 1.6 add_convert_fusion
  (100 shorter events, 11.3 us)
Async XLA Ops:
  7.2 10.6 %copy-start = (bf16[24,1,64,1024]{3,2,1,0:T(8,128)(2,1)S(1)}, bf16[24,1,64,1024]{3,2,1,0:T(8,128)(2,1)}, u32[]{:S(2)}) copy-start(bf16[24,1,64,1024]{3,2,1,0:T(8,128)(2,1)} %param.33) | copy-start | bytes 9437188
  7.2 8.6 %copy-start.2 = (bf16[24,2048]{1,0:T(8,128)(2,1)S(1)}, bf16[24,2048]{1,0:T(8,128)(2,1)}, u32[]{:S(2)}) copy-start(bf16[24,2048]{1,0:T(8,128)(2,1)} %param.24) | copy-start | bytes 294916
  7.2 8.4 %copy-start.19 = (bf16[64]{0:T(256)(128)(2,1)S(1)}, bf16[64]{0:T(256)(128)(2,1)}, u32[]{:S(2)}) copy-start(bf16[64]{0:T(256)(128)(2,1)} %param.31) | copy-start | bytes 388
  7.2 8.5 %copy-start.20 = (bf16[64]{0:T(256)(128)(2,1)S(1)}, bf16[64]{0:T(256)(128)(2,1)}, u32[]{:S(2)}) copy-start(bf16[64]{0:T(256)(128)(2,1)} %param.32) | copy-start | bytes 388
  7.2 41.1 %all-reduce.3.cloned.1.call-start = ((), (), s32[]{:S(2)}) async-start(), calls=%async_computation.4 | async-start | bytes 196608 | tf_op jit(solution)/shard_map/psum | solution.py:124
  13.4 6.3 %copy-start.7 = (f32[24,8]{0,1:T(8,128)}, f32[24,8]{0,1:T(8,128)S(1)}, u32[]{:S(2)}) copy-start(f32[24,8]{0,1:T(8,128)S(1)} %fusion.55) | copy-start | bytes 2308
  15.8 3.8 %copy-start.11 = (f32[64]{0:T(128)}, f32[64]{0:T(128)S(1)}, u32[]{:S(2)}) copy-start(f32[64]{0:T(128)S(1)} %convert_element_type.99) | copy-start | bytes 772
  17.4 2.2 copy-start.13
  17.7 3.1 %copy-start.6 = (bf16[2048,128]{1,0:T(8,128)(2,1)S(1)}, bf16[2048,128]{1,0:T(8,128)(2,1)}, u32[]{:S(2)}) copy-start(bf16[2048,128]{1,0:T(8,128)(2,1)} %param.28) | copy-start | bytes 1572868
  19.6 0.9 copy-start.1
  24.9 2.8 %copy-start.8 = (bf16[2048]{0:T(1024)(128)(2,1)S(1)}, bf16[2048]{0:T(1024)(128)(2,1)}, u32[]{:S(2)}) copy-start(bf16[2048]{0:T(1024)(128)(2,1)} %param.38) | copy-start | bytes 12292
  24.9 25.8 %copy-start.10 = (s32[24,2]{0,1:T(2,128)S(1)}, s32[24,2]{0,1:T(2,128)}, u32[]{:S(2)}) copy-start(s32[24,2]{0,1:T(2,128)} %param.43) | copy-start | bytes 580
  27.6 84.9 %all-gather.2.cloned.1.call-start = ((), (), s32[]{:S(2)}) async-start(), calls=%async_computation.6 | async-start | bytes 1671168 | tf_op jit(solution)/shard_map/all_gather | solution.py:128
  49.3 0.6 copy-start.4
  50.6 70.7 %reduce-scatter.3.cloned.1.call-start = ((), (), s32[]{:S(2)}) async-start(), calls=%async_computation.5 | async-start | bytes 589824 | tf_op jit(solution)/shard_map/reduce_scatter | solution.py:160
  79.2 2.2 copy-start.16
  86.4 143.8 %reduce-scatter.5.cloned.1.call-start = ((), (), s32[]{:S(2)}) async-start(), calls=%async_computation.7 | async-start | bytes 3244032 | tf_op jit(solution)/shard_map/reduce_scatter | solution.py:136
  112.6 3.2 %copy-start.17 = (bf16[2048,512]{1,0:T(8,128)(2,1)S(1)}, bf16[2048,512]{1,0:T(8,128)(2,1)}, u32[]{:S(2)}) copy-start(bf16[2048,512]{1,0:T(8,128)(2,1)} %param.41) | copy-start | bytes 6291460
  112.6 3.2 %copy-start.18 = (bf16[384,2048]{1,0:T(8,128)(2,1)S(1)}, bf16[384,2048]{1,0:T(8,128)(2,1)}, u32[]{:S(2)}) copy-start(bf16[384,2048]{1,0:T(8,128)(2,1)} %all-gather.2.cloned.1.call-done) | copy-start | bytes 4718596
  115.8 1.6 copy-start.3
  120.1 0.7 copy-start.9
  120.1 9.9 %copy-start.12 = (f32[64]{0:T(128)S(1)}, f32[64]{0:T(128)}, u32[]{:S(2)}) copy-start(f32[64]{0:T(128)} %copy-done.11) | copy-start | bytes 772
  120.1 9.9 %copy-start.14 = (f32[24,1]{0,1:T(1,128)S(1)}, f32[24,1]{0,1:T(1,128)}, u32[]{:S(2)}) copy-start(f32[24,1]{0,1:T(1,128)} %copy-done.13) | copy-start | bytes 292
  120.1 10.5 %copy-start.5 = (bf16[24,2048]{1,0:T(8,128)(2,1)S(1)}, bf16[24,2048]{1,0:T(8,128)(2,1)}, u32[]{:S(2)}) copy-start(bf16[24,2048]{1,0:T(8,128)(2,1)} %copy-done.4) | copy-start | bytes 294916
  120.1 21.0 %copy-start.15 = (f32[24,2]{0,1:T(2,128)S(1)}, f32[24,2]{0,1:T(2,128)}, u32[]{:S(2)}) copy-start(f32[24,2]{0,1:T(2,128)} %param.44) | copy-start | bytes 580
  123.1 17.1 %all-to-all-start.1 = ((bf16[16,6,1024]{2,1,0:T(8,128)(2,1)}), bf16[16,6,1024]{2,1,0:T(8,128)(2,1)S(1)}, u32[]{:S(2)}, u32[]{:S(2)}) async-start(bf16[16,6,1024]{2,1,0:T(8,128)(2,1)} %copy.67), calls=%async_computation.2 | async-start | bytes 524288 | tf_op jit(solution)/shard_map/all_to_all | solution.py:163
Sparse Core Ops, SparseCore 0:
  27.8 20.5 all-reduce.2
  51.1 61.4 all-gather.1
  114.8 6.5 reduce-scatter.2
  126.7 103.4 reduce-scatter.4
where the time goes:
time: 240 us; the launch traced here: 239 us
  waiting for transfers between devices  104 us (43%)
  blocking collectives  63.3 us (26%)
  matrix products  29.1 us (12%)
  between operations  14.2 us (6%)
  other arithmetic  12.2 us (5%)
  local copies, waits for them, and re-layouts  9.26 us (4%)
  starting transfers between devices  6.92 us (3%)
    reduce_scatter x1, waiting for transfers between devices, body(): lax.psum_scatter(dense_terms.reshape(-1, half_width), ('ep', 'tp'), scatt...  48.7 us
    unnamed x1, blocking collectives  38.9 us
    all_gather x1, waiting for transfers between devices, body(): all_tokens = lax.all_gather(post_norm, 'ep', axis=0, tiled=True)  26.2 us
    all_to_all x1, blocking collectives, body(): lax.all_to_all(outgoing, 'ep', split_axis=0, concat_axis=0, tiled=True)  24.4 us
    psum x1, waiting for transfers between devices, body(): lax.psum(partial_value.astype(jnp.bfloat16), 'tp').astype(jnp.float32)  20.6 us
    all_to_all x1, waiting for transfers between devices, body(): lax.all_to_all(halves, 'ep', split_axis=0, concat_axis=0, tiled=True)  7.95 us
    all_to_all x1, starting transfers between devices, body(): lax.all_to_all(halves, 'ep', split_axis=0, concat_axis=0, tiled=True)  6.76 us
    dot_general x2, matrix products, swiglu_rows(): jnp.dot(inputs, gate_weight, preferred_element_type=jnp.float32)  5.38 us
  transfers between devices with their start and end apart: 5, of which 5 were waited for; matrix products, arithmetic and copies ran while one was open for 10% of the time, Pallas kernels for 0%

commit v1 on v0

--- a/solution.py
+++ b/solution.py
@@ -121,7 +121,9 @@
     )
     attn_heads = mixed_heads.reshape(seq_count, heads_local * head_size).astype(jnp.bfloat16)
     partial_value = jnp.dot(attn_heads, out_w, preferred_element_type=jnp.float32)
-    attn_sum = lax.psum(partial_value.astype(jnp.bfloat16), "tp").astype(jnp.float32)
+    attn_sum = jnp.sum(lax.all_gather(partial_value.astype(jnp.bfloat16), "tp"), axis=0).astype(
+        jnp.float32
+    )
     resid_out = rounded(resid_in + attn_sum)
     post_norm = rms_scale(resid_out, post_gain.astype(jnp.float32)).astype(jnp.bfloat16)
     branch = jax.nn.sigmoid(jnp.dot(post_norm, branch_gate, preferred_element_type=jnp.float32))

time: 240 us -> 216 us (0.900)
  waiting for transfers between devices: 104 us -> 77.8 us
  blocking collectives: 63.3 us -> 66.1 us
  starting transfers between devices: 6.92 us -> 4.46 us
    psum x1 -> x0, waiting for transfers between devices: 20.6 us -> none  [body(): lax.psum(partial_value.astype(jnp.bfloat16), 'tp').astype(jnp.float32)]
    reduce_scatter x1, waiting for transfers between devices: 48.7 us -> 44.4 us  [body(): lax.psum_scatter(dense_terms.reshape(-1, half_width), ('ep', 'tp'), scatt...]
    all_to_all x1, starting transfers between devices: 6.76 us -> 4.33 us  [body(): lax.all_to_all(halves, 'ep', split_axis=0, concat_axis=0, tiled=True)]
  transfers between devices with their start and end apart: 5 -> 4, of which waited for: 5 -> 3; matrix products, arithmetic and copies ran while one was open for 10% -> 11% of each run, Pallas kernels for 0% -> 0%
where the time goes in v1:
time: 216 us; the launch traced here: 215 us
  waiting for transfers between devices  77.8 us (36%)
  blocking collectives  66.1 us (31%)
  matrix products  27.5 us (13%)
  between operations  16 us (7%)
  other arithmetic  14 us (6%)
  local copies, waits for them, and re-layouts  9.46 us (4%)
  starting transfers between devices  4.46 us (2%)
    reduce_scatter x1, waiting for transfers between devices, body(): lax.psum_scatter(dense_terms.reshape(-1, half_width), ('ep', 'tp'), scatt...  44.4 us
    unnamed x1, blocking collectives  38.7 us
    all_gather x1, waiting for transfers between devices, body(): all_tokens = lax.all_gather(post_norm, 'ep', axis=0, tiled=True)  25.6 us
    all_to_all x1, blocking collectives, body(): lax.all_to_all(outgoing, 'ep', split_axis=0, concat_axis=0, tiled=True)  25.3 us
    all_to_all x1, waiting for transfers between devices, body(): lax.all_to_all(halves, 'ep', split_axis=0, concat_axis=0, tiled=True)  7.67 us
    dot_general x2, matrix products, swiglu_rows(): jnp.dot(inputs, gate_weight, preferred_element_type=jnp.float32)  5.38 us
    all_to_all x1, starting transfers between devices, body(): lax.all_to_all(halves, 'ep', split_axis=0, concat_axis=0, tiled=True)  4.33 us
  transfers between devices with their start and end apart: 4, of which 3 were waited for; matrix products, arithmetic and copies ran while one was open for 11% of the time, Pallas kernels for 0%

profile of v1, /device:TPU:0, one launch (start us, length us, event | category | flops | bytes accessed | tf_op | source)
XLA Modules:
  0.0 215.2 jit_solution(17143496430903450395)
XLA Ops:
  8.9 0.9 iota_compare_fusion.1
  9.8 1.3 convert_element_type.116
  11.2 1.3 select_reduce_fusion
  13.3 1.0 fusion.41
  14.3 1.2 fusion.68
  15.6 2.1 fusion.66
  17.9 1.3 fusion.63
  19.9 1.9 fusion.69
  23.9 3.1 %fusion.30 = bf16[24,8,64]{2,1,0:T(8,128)(2,1)S(1)} fusion(bf16[24,1,64,1024]{3,2,1,0:T(8,128)(2,1)} %param.34, f32[24,8,1024]{2,1,0:T(8,128)} %copy-done.1, f32[24,8]{1,0:T(8,128)S(1)} %get-tuple-element.9, f32[24,8]{1,0:T(8,128)S(1)} %multiply_maximum_fusion, f32[24,64]{1,0:T(8,128)S(1)} %get-tuple-element.4, f32[24,8]{1,0:T(8,128)S(1)} %get-tuple-element.8), kind=kOutput, calls=%fused_computation.24 | convolution fusion | flops 25792512 | bytes 3965184 | tf_op jit(solution)/shard_map/sgrl,sgdl->sgrd/dot_general | solution.py:115
  27.1 2.0 convolution_convert_fusion.2
  29.1 2.1 all-gather
  31.9 1.4 multiply_convert_fusion
  34.9 1.2 fusion.71
  36.0 0.9 reshape.193
  37.0 25.3 %all_to_all.10 = bf16[16,6,2048]{2,1,0:T(8,128)(2,1)} all-to-all(bf16[16,6,2048]{2,1,0:T(8,128)(2,1)} %reshape.193), channel_id=1, replica_groups=mesh['ep'=16,'tp'=2] {'ep'}, dimensions={0} | all-to-all | bytes 786432 | tf_op jit(solution)/shard_map/all_to_all | solution.py:156
  62.3 1.2 reshape.194
  63.4 2.2 %fusion.9 = f32[96,512]{1,0:T(8,128)S(1)} fusion(bf16[96,2048]{1,0:T(8,128)(2,1)S(1)} %reshape.194, bf16[1,2048,512]{2,1,0:T(8,128)(2,1)} %param.45), kind=kOutput, calls=%fused_computation.13 | convolution fusion | flops 201326592 | bytes 2686976 | tf_op jit(solution)/shard_map/dot_general | solution.py:21
  65.7 1.1 fusion.24
  66.8 0.9 dot_general.64
  67.7 2.8 %convolution_convert_fusion = bf16[16,6,2048]{2,0,1:T(8,128)(2,1)} fusion(bf16[1,512,2048]{2,1,0:T(8,128)(2,1)} %param.47, bf16[16,6,512]{2,1,0:T(8,128)(2,1)S(1)} %dot_general.64), kind=kOutput, calls=%fused_computation.4 | convolution fusion | flops 201523200 | bytes 2588672 | tf_op jit(solution)/shard_map/dot_general | solution.py:160
  70.6 25.6 %all-gather.3.cloned.1.call-done = bf16[384,2048]{1,0:T(8,128)(2,1)} async-done(((bf16[24,2048]{1,0:T(8,128)(2,1)}), bf16[384,2048]{1,0:T(8,128)(2,1)}) %all-gather.3.cloned.1.call-update) | async-done | bytes 1572880 | tf_op jit(solution)/shard_map/all_gather | solution.py:130
  96.2 3.2 %fusion.70 = f32[384,512]{1,0:T(8,128)S(1)} fusion(bf16[384,2048]{1,0:T(8,128)(2,1)} %all-gather.3.cloned.1.call-done, bf16[2048,512]{1,0:T(8,128)(2,1)} %param.40), kind=kOutput, calls=%fused_computation.98 | convolution fusion | flops 805306368 | bytes 4456448 | tf_op jit(solution)/shard_map/dot_general | solution.py:21
  99.4 1.1 multiply_reduce_fusion
  101.0 2.7 %fusion.4 = f32[16,24,2,1024]{3,1,2,0:T(8,128)} fusion(bf16[16,24,512,1]{2,1,3,0:T(8,128)(2,1)S(1)} %bitcast.87, bf16[64,2,8,1024]{3,2,1,0:T(8,128)(2,1)S(1)} %bitcast.85), kind=kOutput, calls=%fused_computation.8 | convolution fusion | flops 805306368 | bytes 5636096 | tf_op jit(solution)/shard_map/esh,hcd->ecsd/dot_general | solution.py:29
  105.3 1.8 copy.67
  107.1 4.3 %all-to-all-start.1 = ((bf16[16,6,1024]{2,1,0:T(8,128)(2,1)}), bf16[16,6,1024]{2,1,0:T(8,128)(2,1)S(1)}, u32[]{:S(2)}, u32[]{:S(2)}) async-start(bf16[16,6,1024]{2,1,0:T(8,128)(2,1)} %copy.67), calls=%async_computation.2 | async-start | bytes 524288 | tf_op jit(solution)/shard_map/all_to_all | solution.py:165
  112.2 7.7 %all-to-all-done.1 = bf16[16,6,1024]{2,1,0:T(8,128)(2,1)S(1)} async-done(((bf16[16,6,1024]{2,1,0:T(8,128)(2,1)}), bf16[16,6,1024]{2,1,0:T(8,128)(2,1)S(1)}, u32[]{:S(2)}, u32[]{:S(2)}) %all-to-all-start.1) | async-done | bytes 196640 | tf_op jit(solution)/shard_map/all_to_all | solution.py:165
  120.7 1.2 fusion.23
  122.0 38.7 %all-reduce = f32[768]{0:T(1024)S(1)} all-reduce(f32[768]{0:T(1024)S(1)} %reshape.199), channel_id=5, replica_groups=mesh['ep'=16,'tp'=2] {'ep','tp'}, use_global_device_ids=true, to_apply=%region_15.16.clone | all-reduce | flops 768 | bytes 6144
  160.8 44.4 %reduce-scatter.5.cloned.1.call-done = f32[24,1024]{1,0:T(8,128)} async-done(((f32[768,1024]{1,0:T(8,128)}), f32[24,1024]{1,0:T(8,128)}) %reduce-scatter.5.cloned.1.call-update) | async-done | bytes 98320 | tf_op jit(solution)/shard_map/reduce_scatter | solution.py:138
  205.2 1.0 multiply_convert_fusion.1
  206.2 1.6 add_convert_fusion
  (99 shorter events, 11.0 us)
Async XLA Ops:
  8.0 11.8 %copy-start = (bf16[24,1,64,1024]{3,2,1,0:T(8,128)(2,1)S(1)}, bf16[24,1,64,1024]{3,2,1,0:T(8,128)(2,1)}, u32[]{:S(2)}) copy-start(bf16[24,1,64,1024]{3,2,1,0:T(8,128)(2,1)} %param.33) | copy-start | bytes 9437188
  8.0 9.9 %copy-start.2 = (bf16[24,2048]{1,0:T(8,128)(2,1)S(1)}, bf16[24,2048]{1,0:T(8,128)(2,1)}, u32[]{:S(2)}) copy-start(bf16[24,2048]{1,0:T(8,128)(2,1)} %param.24) | copy-start | bytes 294916
  8.0 9.7 %copy-start.19 = (bf16[64]{0:T(256)(128)(2,1)S(1)}, bf16[64]{0:T(256)(128)(2,1)}, u32[]{:S(2)}) copy-start(bf16[64]{0:T(256)(128)(2,1)} %param.31) | copy-start | bytes 388
  8.0 9.8 %copy-start.20 = (bf16[64]{0:T(256)(128)(2,1)S(1)}, bf16[64]{0:T(256)(128)(2,1)}, u32[]{:S(2)}) copy-start(bf16[64]{0:T(256)(128)(2,1)} %param.32) | copy-start | bytes 388
  8.0 88.2 %all-gather.3.cloned.1.call-start = ((), (), s32[]{:S(2)}) async-start(), calls=%async_computation.5 | async-start | bytes 1671168 | tf_op jit(solution)/shard_map/all_gather | solution.py:130
  15.5 6.3 %copy-start.8 = (f32[24,8]{0,1:T(8,128)}, f32[24,8]{0,1:T(8,128)S(1)}, u32[]{:S(2)}) copy-start(f32[24,8]{0,1:T(8,128)S(1)} %fusion.55) | copy-start | bytes 2308
  17.9 3.8 %copy-start.11 = (f32[64]{0:T(128)}, f32[64]{0:T(128)S(1)}, u32[]{:S(2)}) copy-start(f32[64]{0:T(128)S(1)} %convert_element_type.101) | copy-start | bytes 772
  19.5 2.2 %copy-start.13 = (f32[24,1]{0,1:T(1,128)}, f32[24,1]{0,1:T(1,128)S(1)}, u32[]{:S(2)}) copy-start(f32[24,1]{0,1:T(1,128)S(1)} %constant_dynamic-slice_fusion.2) | copy-start | bytes 292
  19.8 3.1 %copy-start.7 = (bf16[2048,128]{1,0:T(8,128)(2,1)S(1)}, bf16[2048,128]{1,0:T(8,128)(2,1)}, u32[]{:S(2)}) copy-start(bf16[2048,128]{1,0:T(8,128)(2,1)} %param.28) | copy-start | bytes 1572868
  21.7 0.9 copy-start.1
  27.0 6.4 %copy-start.10 = (s32[24,2]{0,1:T(2,128)S(1)}, s32[24,2]{0,1:T(2,128)}, u32[]{:S(2)}) copy-start(s32[24,2]{0,1:T(2,128)} %param.43) | copy-start | bytes 580
  31.2 0.6 copy-start.4
  33.3 72.0 %reduce-scatter.3.cloned.1.call-start = ((), (), s32[]{:S(2)}) async-start(), calls=%async_computation.4 | async-start | bytes 589824 | tf_op jit(solution)/shard_map/reduce_scatter | solution.py:162
  63.4 2.2 %copy-start.16 = (bf16[1,2048,512]{2,1,0:T(8,128)(2,1)S(1)}, bf16[1,2048,512]{2,1,0:T(8,128)(2,1)}, u32[]{:S(2)}) copy-start(bf16[1,2048,512]{2,1,0:T(8,128)(2,1)} %param.46) | copy-start | bytes 6291460
  70.5 134.7 %reduce-scatter.5.cloned.1.call-start = ((), (), s32[]{:S(2)}) async-start(), calls=%async_computation.6 | async-start | bytes 3244032 | tf_op jit(solution)/shard_map/reduce_scatter | solution.py:138
  96.2 3.2 %copy-start.17 = (bf16[2048,512]{1,0:T(8,128)(2,1)S(1)}, bf16[2048,512]{1,0:T(8,128)(2,1)}, u32[]{:S(2)}) copy-start(bf16[2048,512]{1,0:T(8,128)(2,1)} %param.41) | copy-start | bytes 6291460
  96.2 3.2 %copy-start.18 = (bf16[384,2048]{1,0:T(8,128)(2,1)S(1)}, bf16[384,2048]{1,0:T(8,128)(2,1)}, u32[]{:S(2)}) copy-start(bf16[384,2048]{1,0:T(8,128)(2,1)} %all-gather.3.cloned.1.call-done) | copy-start | bytes 4718596
  99.4 1.6 copy-start.3
  103.7 0.9 copy-start.5
  103.7 1.6 copy-start.9
  103.7 7.7 %copy-start.12 = (f32[64]{0:T(128)S(1)}, f32[64]{0:T(128)}, u32[]{:S(2)}) copy-start(f32[64]{0:T(128)} %copy-done.11) | copy-start | bytes 772
  103.7 7.7 %copy-start.14 = (f32[24,1]{0,1:T(1,128)S(1)}, f32[24,1]{0,1:T(1,128)}, u32[]{:S(2)}) copy-start(f32[24,1]{0,1:T(1,128)} %copy-done.13) | copy-start | bytes 292
  103.7 8.4 %copy-start.6 = (bf16[24,2048]{1,0:T(8,128)(2,1)S(1)}, bf16[24,2048]{1,0:T(8,128)(2,1)}, u32[]{:S(2)}) copy-start(bf16[24,2048]{1,0:T(8,128)(2,1)} %multiply_convert_fusion) | copy-start | bytes 294916
  103.7 17.0 %copy-start.15 = (f32[24,2]{0,1:T(2,128)S(1)}, f32[24,2]{0,1:T(2,128)}, u32[]{:S(2)}) copy-start(f32[24,2]{0,1:T(2,128)} %param.44) | copy-start | bytes 580
  107.1 12.8 %all-to-all-start.1 = ((bf16[16,6,1024]{2,1,0:T(8,128)(2,1)}), bf16[16,6,1024]{2,1,0:T(8,128)(2,1)S(1)}, u32[]{:S(2)}, u32[]{:S(2)}) async-start(bf16[16,6,1024]{2,1,0:T(8,128)(2,1)} %copy.67), calls=%async_computation.2 | async-start | bytes 524288 | tf_op jit(solution)/shard_map/all_to_all | solution.py:165
Sparse Core Ops, SparseCore 0:
  33.4 62.7 all-gather.2
Sparse Core Ops, SparseCore 1:
  70.6 6.5 reduce-scatter.2
  103.8 101.4 reduce-scatter.4
